TPU v7x, 32 devices: a whole 2x2x4 slice. The times are simulated.
32 devices in a mesh: fs: 8 (over z, x), tp: 4 (over y, core).
Axes of the slice: x: 2, y: 2, z: 4, core: 2. Of those that a mesh axis runs over, the one named last changes fastest.
Arguments:
- tokens: bfloat16 [2048, 2048], P('fs'), may hold values from -6 to 6
- norm_gain: float32 [2048], P('fs'), may hold values from 0.1 to 1.9
- gate_weight: float32 [8, 2048, 2048], P(None, 'fs', 'tp'), as said below
- up_weight: float32 [8, 2048, 2048], P(None, 'fs', 'tp'), as said below
- down_weight: float32 [8, 2048, 2048], P(None, 'fs', 'tp'), may hold values from -0.125 to 0.125
- routes: int32 [2048, 4], P('fs'), may hold values from 0 to 7, all different within a row; in each aligned block of 256 rows (0 to 255, 256 to 511, ...) at most 192 rows name the same one
- route_weights: bfloat16 [2048, 4], P('fs'), may hold values from 0.049804688 to 0.59765625
Outputs:
- gate_ready: bfloat16 [8, 2048, 2048], P('fs', None, 'tp')
- up_ready: bfloat16 [8, 2048, 2048], P('fs', None, 'tp')
- down_ready: bfloat16 [8, 2048, 2048], P('fs', None, 'tp')
- moe_output: bfloat16 [2048, 2048], P('fs', 'tp')
Inputs may be any that keep to these rules, and one draw needn't show every extreme that they name: `routes`: each row names 4 different experts; among the rows of one index of fs no expert is named more than 192 times. `gate_weight`: real-valued entries, drawn afresh for each expert; the scale may differ from column to column. `up_weight`: real-valued entries, drawn afresh for each expert; the scale may differ from column to column.
All inputs are finite; a program needn't handle non-finite values.
Results may differ from a plain program's by a relative error of at most 0.015.
Values may be sent and summed in bfloat16 or wider, within the bound.
A program may use at most 128 MiB of HBM per device.

v0:
```python
import functools

import jax
import jax.numpy as jnp
from jax import lax
from jax.experimental import pallas as pl
from jax.experimental.pallas import tpu as pltpu
from jax.sharding import PartitionSpec as P

norm_eps = 1e-06
clamp_limit = 7.0
gate_alpha = 1.702
MESH = pl.DeviceIdType.MESH
CORES = 2
DEPTH = 4


def activate(gate_pre, up_pre):
    gate_part = jnp.minimum(gate_pre, clamp_limit)
    up_part = jnp.clip(up_pre, -clamp_limit, clamp_limit)
    return (up_part + 1.0) * gate_part * jax.nn.sigmoid(gate_alpha * gate_part)


def earlier_counts(member):
    rows = member.shape[1]
    before = (
        jnp.arange(rows, dtype=jnp.int32)[:, None] < jnp.arange(rows, dtype=jnp.int32)[None, :]
    ).astype(jnp.bfloat16)
    return jnp.dot(
        member.astype(jnp.bfloat16), before, preferred_element_type=jnp.float32
    ).astype(jnp.int32)


def kernel(
    n,
    groups,
    row_tile,
    sent,
    gain,
    gate_local,
    up_local,
    down_local,
    gate_ready,
    up_ready,
    down_ready,
    returned,
    routed,
    hidden,
    kept,
    given,
    partner_sums,
    chip_sums,
    finished,
    wide,
    staged,
    dispatch_send,
    dispatch_recv,
    share_send,
    share_recv,
    weight_send,
    weight_recv,
    pair_send,
    pair_recv,
    chip_send,
    chip_recv,
    return_send,
    return_recv,
    own_sem,
    wide_sem,
):
    me = lax.axis_index("fs")
    tp = lax.axis_index("tp")
    chips = groups // CORES
    chip = tp // CORES
    core = lax.rem(tp, CORES)
    partner = chip * CORES + (CORES - 1 - core)
    capacity = sent.shape[0] // n
    source_rows = gate_local.shape[1]
    part = sent.shape[1]
    shares = n // groups
    total_slots = n * capacity

    def slots_of(block):
        return pl.ds(pl.multiple_of(block * capacity, 16), capacity)

    def rows_of(block):
        return pl.ds(pl.multiple_of(block * source_rows, 16), source_rows)

    locals_ = (gate_local, up_local, down_local)
    readies = (gate_ready, up_ready, down_ready)
    blocks = [(j, k) for turn in ((0, 1), (2,)) for k in range(n) for j in turn]

    def fetch(i):
        j, k = blocks[i]
        copy = pltpu.make_async_copy(
            locals_[j].at[lax.rem(me + k, n)], wide.at[i % DEPTH], wide_sem.at[i % DEPTH]
        )
        copy.start()
        return copy

    fetches = [fetch(i) for i in range(DEPTH)]

    barrier = pltpu.get_barrier_semaphore()
    for k in range(1, n):
        pl.semaphore_signal(
            barrier, inc=1, device_id=(lax.rem(me + k, n), tp), device_id_type=MESH
        )
    for k in range(1, groups):
        pl.semaphore_signal(
            barrier, inc=1, device_id=(me, lax.rem(tp + k, groups)), device_id_type=MESH
        )
    pl.semaphore_wait(barrier, n + groups - 2)

    waits = []

    dispatch = {}
    for k in range(1, n):
        peer = lax.rem(me + k, n)
        copy = pltpu.make_async_remote_copy(
            src_ref=sent.at[slots_of(peer)],
            dst_ref=routed.at[tp, slots_of(me)],
            send_sem=dispatch_send.at[k],
            recv_sem=dispatch_recv.at[k],
            device_id=(peer, tp),
            device_id_type=MESH,
        )
        copy.start()
        dispatch[k] = copy
    own_tokens = pltpu.make_async_copy(
        sent.at[slots_of(me)], routed.at[tp, slots_of(me)], own_sem.at[0]
    )
    own_tokens.start()
    own_copies = []
    weights = {}

    def send(j, k):
        copy = pltpu.make_async_remote_copy(
            src_ref=staged.at[j, k - 1],
            dst_ref=readies[j].at[rows_of(me)],
            send_sem=weight_send.at[j, k],
            recv_sem=weight_recv.at[j, k],
            device_id=(lax.rem(me + k, n), tp),
            device_id_type=MESH,
        )
        copy.start()
        weights[j, k] = copy

    for i, (j, k) in enumerate(blocks):
        fetches[i].wait()
        value = wide[i % DEPTH]
        if j < 2:
            value = gain[...] * value
        if k == 0:
            readies[j][rows_of(me), :] = value.astype(jnp.bfloat16)
        else:
            staged[j, k - 1] = value.astype(jnp.bfloat16)
        if i + DEPTH < len(blocks):
            fetches.append(fetch(i + DEPTH))
        if i > 0 and blocks[i - 1][1] > 0:
            send(*blocks[i - 1])
    send(*blocks[-1])

    for k in range(n):
        source = lax.rem(me - k + n, n)
        if k == 0:
            own_tokens.wait()
        else:
            dispatch[k].wait_recv()
        for step in range(1, groups):
            pltpu.make_async_remote_copy(
                src_ref=routed.at[tp, slots_of(source)],
                dst_ref=routed.at[tp, slots_of(source)],
                send_sem=share_send.at[step],
                recv_sem=share_recv.at[step],
                device_id=(me, lax.rem(tp + step, groups)),
                device_id_type=MESH,
            ).start()
    share_waits = []
    for step in range(1, groups):
        origin = lax.rem(tp - step + groups, groups)
        share = pltpu.make_async_remote_copy(
            src_ref=routed.at[tp],
            dst_ref=routed.at[origin],
            send_sem=share_send.at[step],
            recv_sem=share_recv.at[step],
            device_id=(me, lax.rem(tp + step, groups)),
            device_id_type=MESH,
        )
        share.wait_recv()
        share_waits.append(share)

    for j in range(2):
        for k in range(1, n):
            weights[j, k].wait_recv()

    @pl.loop(0, total_slots // row_tile)
    def _(tile):
        rows = pl.ds(pl.multiple_of(tile * row_tile, 16), row_tile)
        gate_pre = jnp.zeros((row_tile, hidden.shape[1]), jnp.float32)
        up_pre = jnp.zeros((row_tile, hidden.shape[1]), jnp.float32)
        for t in range(groups):
            piece = routed[t, rows, :]
            gate_pre += jnp.dot(
                piece, gate_ready[t * part : (t + 1) * part], preferred_element_type=jnp.float32
            )
            up_pre += jnp.dot(
                piece, up_ready[t * part : (t + 1) * part], preferred_element_type=jnp.float32
            )
        hidden[rows, :] = activate(gate_pre, up_pre).astype(jnp.bfloat16)

    def arrival(source):
        k = lax.rem(me - source + n, n)

        @pl.when(k > 0)
        def _():
            pltpu.make_async_remote_copy(
                src_ref=staged.at[2, 0],
                dst_ref=down_ready.at[rows_of(source)],
                send_sem=weight_send.at[2, k],
                recv_sem=weight_recv.at[2, k],
                device_id=(me, partner),
                device_id_type=MESH,
            ).wait_recv()

    def project(source, out, slot):
        down = down_ready[rows_of(source), :]

        @pl.loop(0, total_slots // row_tile)
        def _(tile):
            rows = pl.ds(pl.multiple_of(tile * row_tile, 16), row_tile)
            out[slot, rows, :] = lax.dot_general(
                hidden[rows, :], down, (((1,), (1,)), ((), ())), preferred_element_type=jnp.float32
            ).astype(jnp.bfloat16)

    sums = []
    order = [(h, r) for h in range(1, chips) for r in range(shares)]
    order += [(0, r) for r in range(shares)]

    def start_group(h, r):
        slot = h * shares + r
        to_chip = lax.rem(chip + h, chips)
        give_source = (to_chip * CORES + (CORES - 1 - core)) * shares + r
        keep_source = (to_chip * CORES + core) * shares + r
        arrival(give_source)
        project(give_source, given, slot)
        pair = pltpu.make_async_remote_copy(
            src_ref=given.at[slot],
            dst_ref=partner_sums.at[slot],
            send_sem=pair_send.at[slot],
            recv_sem=pair_recv.at[slot],
            device_id=(me, partner),
            device_id_type=MESH,
        )
        pair.start()
        arrival(keep_source)
        project(keep_source, kept, slot)
        return pair

    for h, r in order:
        slot = h * shares + r
        pair = start_group(h, r)
        pair.wait_recv()
        waits.append(pair)
        if h > 0:

            @pl.loop(0, total_slots // row_tile)
            def _(tile):
                rows = pl.ds(pl.multiple_of(tile * row_tile, 16), row_tile)
                total = kept[slot, rows, :].astype(jnp.float32)
                total += partner_sums[slot, rows, :].astype(jnp.float32)
                kept[slot, rows, :] = total.astype(jnp.bfloat16)

            over = pltpu.make_async_remote_copy(
                src_ref=kept.at[slot],
                dst_ref=chip_sums.at[slot - shares],
                send_sem=chip_send.at[slot - shares],
                recv_sem=chip_recv.at[slot - shares],
                device_id=(me, lax.rem(chip + h, chips) * CORES + core),
                device_id_type=MESH,
            )
            over.start()
            sums.append((r, over))
            waits.append(over)
        else:
            for share, over in sums:
                if share == r:
                    over.wait_recv()

            @pl.loop(0, total_slots // row_tile)
            def _(tile):
                rows = pl.ds(pl.multiple_of(tile * row_tile, 16), row_tile)
                total = kept[slot, rows, :].astype(jnp.float32)
                total += partner_sums[slot, rows, :].astype(jnp.float32)
                for other in range(1, chips):
                    total += chip_sums[(other - 1) * shares + r, rows, :].astype(jnp.float32)
                finished[r, rows, :] = total.astype(jnp.bfloat16)

            for k in range(1, n):
                peer = lax.rem(me + k, n)
                back = pltpu.make_async_remote_copy(
                    src_ref=finished.at[r, slots_of(peer)],
                    dst_ref=returned.at[r, slots_of(me)],
                    send_sem=return_send.at[r, k],
                    recv_sem=return_recv.at[r, k],
                    device_id=(peer, tp),
                    device_id_type=MESH,
                )
                back.start()
                waits.append(back)
                sums.append((-1, back))
            own = pltpu.make_async_copy(
                finished.at[r, slots_of(me)], returned.at[r, slots_of(me)], own_sem.at[1 + r]
            )
            own.start()
            own_copies.append(own)

    for share, back in sums:
        if share == -1:
            back.wait_recv()
    for own in own_copies:
        own.wait()
    for copy in waits + share_waits + list(dispatch.values()) + list(weights.values()):
        copy.wait_send()


def hand_over(sent, gain, gate_local, up_local, down_local):
    n = lax.axis_size("fs")
    groups = lax.axis_size("tp")
    total_slots, part = sent.shape
    source_rows, units = gate_local.shape[1:]
    width = n * source_rows
    shares = n // groups
    chips = groups // CORES
    vmem = pl.BlockSpec(memory_space=pltpu.VMEM)
    anywhere = pl.BlockSpec(memory_space=pl.ANY)
    bf16 = jnp.bfloat16
    ready = jax.ShapeDtypeStruct((width, units), bf16)
    dma = pltpu.SemaphoreType.DMA
    return pl.pallas_call(
        functools.partial(kernel, n, groups, total_slots // 4),
        out_shape=(
            ready,
            ready,
            ready,
            jax.ShapeDtypeStruct((shares, total_slots, source_rows), bf16),
        ),
        in_specs=[anywhere, vmem] + [anywhere] * 3,
        out_specs=(vmem,) * 4,
        scratch_shapes=[
            pltpu.VMEM((groups, total_slots, part), bf16),
            pltpu.VMEM((total_slots, units), bf16),
            pltpu.VMEM((chips * shares, total_slots, source_rows), bf16),
            pltpu.VMEM((chips * shares, total_slots, source_rows), bf16),
            pltpu.VMEM((chips * shares, total_slots, source_rows), bf16),
            pltpu.VMEM(((chips - 1) * shares, total_slots, source_rows), bf16),
            pltpu.VMEM((shares, total_slots, source_rows), bf16),
            pltpu.VMEM((DEPTH, source_rows, units), jnp.float32),
            pltpu.VMEM((3, n - 1, source_rows, units), bf16),
            dma((n,)),
            dma((n,)),
            dma((groups,)),
            dma((groups,)),
            dma((3, n)),
            dma((3, n)),
            dma((chips * shares,)),
            dma((chips * shares,)),
            dma(((chips - 1) * shares,)),
            dma(((chips - 1) * shares,)),
            dma((shares, n)),
            dma((shares, n)),
            dma((1 + shares,)),
            dma((DEPTH,)),
        ],
        compiler_params=pltpu.CompilerParams(
            collective_id=0, has_side_effects=True, vmem_limit_bytes=52 * 1024 * 1024
        ),
    )(sent, gain, gate_local, up_local, down_local)


def body(tokens, norm_gain, gate_weight, up_weight, down_weight, routes, route_weights):
    experts = lax.axis_size("fs")
    groups = lax.axis_size("tp")
    tok_rows, model_width = tokens.shape
    top_count = routes.shape[1]
    capacity = 3 * tok_rows * top_count // (2 * experts)
    total_slots = experts * capacity
    part_width = model_width // groups

    wide_tokens = tokens.astype(jnp.float32)
    scale = lax.rsqrt(jnp.mean(wide_tokens * wide_tokens, axis=1, keepdims=True) + norm_eps)
    start = lax.axis_index("tp") * part_width
    columns = (
        lax.dynamic_slice_in_dim(tokens, start, part_width, 1).astype(jnp.float32) * scale
    ).astype(jnp.bfloat16)

    chosen = routes.T[:, None, :] == jnp.arange(experts, dtype=jnp.int32)[None, :, None]
    member = jnp.sum(chosen.astype(jnp.int32), axis=0)
    position = jnp.where(member > 0, earlier_counts(member), -1)
    row_weight = jnp.sum(
        jnp.where(chosen, route_weights.T.astype(jnp.float32)[:, None, :], 0.0), axis=0
    )
    here = position[:, None, :] == jnp.arange(capacity, dtype=jnp.int32)[None, :, None]
    pick = here.astype(jnp.bfloat16).reshape(total_slots, tok_rows)
    table = (
        jnp.where(here, row_weight[:, None, :], jnp.float32(0.0))
        .astype(jnp.bfloat16)
        .reshape(total_slots, tok_rows)
    )
    sent = jnp.dot(pick, columns, preferred_element_type=jnp.float32).astype(jnp.bfloat16)

    gate_ready, up_ready, down_ready, returned = hand_over(
        sent, norm_gain[:, None], gate_weight, up_weight, down_weight
    )
    moe_output = jnp.concatenate(
        [
            lax.dot_general(
                table, piece, (((0,), (0,)), ((), ())), preferred_element_type=jnp.float32
            ).astype(jnp.bfloat16)
            for piece in returned
        ],
        axis=1,
    )
    return (gate_ready[None], up_ready[None], down_ready[None], moe_output)


def solution(mesh):
    in_specs = (
        P("fs", None),
        P("fs"),
        P(None, "fs", "tp"),
        P(None, "fs", "tp"),
        P(None, "fs", "tp"),
        P("fs", None),
        P("fs", None),
    )
    out_specs = (P("fs", None, "tp"), P("fs", None, "tp"), P("fs", None, "tp"), P("fs", "tp"))
    return jax.shard_map(body, mesh=mesh, in_specs=in_specs, out_specs=out_specs, check_vma=False)
```

profile of v0, /device:TPU:19, one launch (start us, length us, event | category | flops | bytes accessed | tf_op | source)
XLA Modules:
  0.0 246.8 jit_solution(8188723395024510664)
XLA Ops:
  0.6 0.0 copy-start.5
  0.6 0.7 convert_reduce_fusion
  1.3 0.2 fusion
  1.5 0.1 eq.55
  1.6 0.3 bitcast_compare_fusion
  1.9 1.5 multiply_reduce_fusion
  3.4 2.8 %convolution_convert_fusion.sent = bf16[1536,512]{1,0:T(8,128)(2,1)} fusion(pred[1536,256]{1,0:T(32,128)(4,1)S(1)} %bitcast_compare_fusion, f32[256]{0:T(256)S(1)} %add_rsqrt_fusion, bf16[256,2048]{1,0:T(8,128)(2,1)} %param.7, s32[]{:T(128)S(6)} %select_n.28), kind=kOutput, calls=%fused_computation | convolution fusion | flops 403832832 | bytes 2229252 | tf_op jit(solution)/shard_map/dot_general | solution.py:409
  6.2 0.0 copy-done.5
  6.2 0.1 copy.14.gain
  6.3 0.0 copy-start.4
  6.3 0.0 copy-start.3
  6.3 232.1 %shard_map.102 = (bf16[2048,512]{1,0:T(8,128)(2,1)}, bf16[2048,512]{1,0:T(8,128)(2,1)}, bf16[2048,512]{1,0:T(8,128)(2,1)}, bf16[2,1536,256]{2,1,0:T(8,128)(2,1)S(1)}) custom-call(bf16[1536,512]{1,0:T(8,128)(2,1)} %convolution_convert_fusion.sent, f32[256,1]{1,0:T(8,128)S(1)} %copy.14.gain, f32[8,256,512]{2,1,0:T(8,128)} %gate_local.1, ...), custom_call_target="tpu_custom_call" | custom-call | tf_op jit(solution)/shard_map/pallas_call | solution.py:339
  238.4 0.0 copy-done.4
  238.4 0.0 copy-done.3
  238.5 0.2 select_convert_fusion
  238.7 0.4 convolution_convert_fusion.1
  239.1 0.0 copy-start.2
  239.2 0.4 convolution_convert_fusion.2
  239.6 0.8 copy.15
  240.5 0.3 copy-done.2
  240.7 0.0 copy-start.1
  240.7 1.3 copy.21
  242.1 1.0 copy-done.1
  243.1 0.0 copy-start
  243.1 1.3 copy.22
  244.4 1.0 copy-done
  245.4 1.3 copy.23
  (5 shorter events, 0.0 us)
Async XLA Ops:
  0.6 5.5 %copy-start.5 = (f32[256]{0:T(256)S(1)}, f32[256]{0:T(256)}, u32[]{:S(2)}) copy-start(f32[256]{0:T(256)} %param.8) | copy-start | bytes 3076
  6.3 232.1 %copy-start.4 = (bf16[256,4]{0,1:T(4,128)(2,1)S(1)}, bf16[256,4]{0,1:T(4,128)(2,1)}, u32[]{:S(2)}) copy-start(bf16[256,4]{0,1:T(4,128)(2,1)} %param.13) | copy-start | bytes 6148
  6.3 232.1 %copy-start.3 = (s32[256,4]{0,1:T(4,128)S(1)}, s32[256,4]{0,1:T(4,128)}, u32[]{:S(2)}) copy-start(s32[256,4]{0,1:T(4,128)} %param.12) | copy-start | bytes 12292
  239.1 1.6 copy-start.2
  240.7 2.3 copy-start.1
  243.1 2.3 copy-start
where the time goes:
time: 247 us
  Pallas kernels  232 us (94%)
  local copies, waits for them, and re-layouts  7.37 us (3%)
  matrix products  3.77 us (2%)
  other arithmetic  2.78 us (1%)
    pallas_call x1, Pallas kernels, hand_over(): pl.pallas_call(functools.partial(kernel, n, groups, total_slots // 4), ou...  232 us
    unnamed x16, local copies, waits for them, and re-layouts  7.15 us

commit v1 on v0

v1 whole, which is shorter than its diff:
```python
import functools

import jax
import jax.numpy as jnp
from jax import lax
from jax.experimental import pallas as pl
from jax.experimental.pallas import tpu as pltpu
from jax.sharding import PartitionSpec as P

norm_eps = 1e-06
clamp_limit = 7.0
gate_alpha = 1.702
MESH = pl.DeviceIdType.MESH
CORES = 2
DEPTH = 6
LANES = 128


def activate(gate_pre, up_pre):
    gate_part = jnp.minimum(gate_pre, clamp_limit)
    up_part = jnp.clip(up_pre, -clamp_limit, clamp_limit)
    return (up_part + 1.0) * gate_part * jax.nn.sigmoid(gate_alpha * gate_part)


def line_width(n):
    width = 1
    while 4 * width * width <= n:
        width *= 2
    return width


def kernel(
    n,
    groups,
    nx,
    row_tile,
    tokens,
    gain,
    routes,
    route_weights,
    gate_local,
    up_local,
    down_local,
    gate_ready,
    up_ready,
    down_ready,
    out,
    wide,
    token_rows,
    staged,
    gathered,
    meta,
    metas,
    tables,
    routed,
    gate_pre,
    hidden,
    given,
    kept,
    partner_sums,
    chip_sums,
    expert_out,
    row_sums,
    x_out,
    x_in,
    near_out,
    near_in,
    far_out,
    far_in,
    cross_out,
    cross_in,
    finished,
    wide_sem,
    token_sem,
    meta_send,
    meta_recv,
    token_send,
    token_recv,
    share_send,
    share_recv,
    forward_send,
    forward_recv,
    weight_send,
    weight_recv,
    down_send,
    down_recv,
    pair_send,
    pair_recv,
    chip_send,
    chip_recv,
    x_send,
    x_recv,
    near_send,
    near_recv,
    far_send,
    far_recv,
    cross_send,
    cross_recv,
):
    me = lax.axis_index("fs")
    tp = lax.axis_index("tp")
    chips = groups // CORES
    chip = tp // CORES
    core = lax.rem(tp, CORES)
    partner = chip * CORES + (CORES - 1 - core)
    nz = n // nx
    span = nz // 2
    z = me // nx
    x = lax.rem(me, nx)
    half = z // span
    local = lax.rem(z, span)
    gate_way = span - 1 + half
    far_way = span - half
    tok_rows, width = token_rows.shape
    part = width // groups
    source_rows = gate_local.shape[1]
    shares = n // groups
    total_slots = hidden.shape[0]
    capacity = total_slots // n
    chunks = given.shape[0]
    piece = source_rows // chunks
    f32, bf16 = jnp.float32, jnp.bfloat16

    def at(zz, xx):
        return zz * nx + xx

    def near(i):
        return half * span + lax.rem(local + i, span)

    def far(i):
        return (1 - half) * span + lax.rem(local + i, span)

    def beside(dx):
        return lax.rem(x + dx, nx)

    def slots_of(block):
        return pl.ds(pl.multiple_of(block * capacity, 16), capacity)

    def rows_of(block):
        return pl.ds(pl.multiple_of(block * source_rows, 16), source_rows)

    def chunk_of(block, i):
        return pl.ds(pl.multiple_of(block * source_rows + i * piece, 16), piece)

    sends = []

    def remote(src, dst, send_sem, recv_sem, device):
        return pltpu.make_async_remote_copy(
            src_ref=src,
            dst_ref=dst,
            send_sem=send_sem,
            recv_sem=recv_sem,
            device_id=device,
            device_id_type=MESH,
        )

    def push(src, dst, send_sem, recv_sem, device, keep=True):
        copy = remote(src, dst, send_sem, recv_sem, device)
        copy.start()
        if keep:
            sends.append(copy)
        return copy

    peers = [at(far(i), beside(dx)) for i in range(span) for dx in range(nx)]
    peers += [at(near(i), beside(dx)) for i in range(span) for dx in range(nx) if i + dx > 0]
    places = peers + [me]
    locals_ = (gate_local, up_local, down_local)
    readies = (gate_ready, up_ready, down_ready)
    blocks = [(j, q) for j in range(3) for q in range(n)]

    def fetch(i):
        j, q = blocks[i]
        copy = pltpu.make_async_copy(
            locals_[j].at[places[q]], wide.at[i % DEPTH], wide_sem.at[i % DEPTH]
        )
        copy.start()
        return copy

    token_copy = pltpu.make_async_copy(tokens, token_rows, token_sem)
    token_copy.start()
    fetches = [fetch(i) for i in range(DEPTH)]

    barrier = pltpu.get_barrier_semaphore()
    for k in range(1, n):
        pl.semaphore_signal(
            barrier, inc=1, device_id=(lax.rem(me + k, n), tp), device_id_type=MESH
        )
    for k in range(1, groups):
        pl.semaphore_signal(
            barrier, inc=1, device_id=(me, lax.rem(tp + k, groups)), device_id_type=MESH
        )

    token_copy.wait()

    @pl.loop(0, tok_rows // 32)
    def _(tile):
        rows = pl.ds(pl.multiple_of(tile * 32, 32), 32)
        wide_rows = token_rows[rows, :].astype(f32)
        scale = lax.rsqrt(jnp.mean(wide_rows * wide_rows, axis=1, keepdims=True) + norm_eps)
        columns = pl.ds(pl.multiple_of(tp * part, LANES), part)
        gathered[me, rows, :] = (token_rows[rows, columns].astype(f32) * scale).astype(bf16)

    ids = lax.broadcasted_iota(jnp.int32, (n, tok_rows), 0)
    member = jnp.zeros((n, tok_rows), f32)
    row_weight = jnp.zeros((n, tok_rows), f32)
    for k in range(routes.shape[0]):
        hit = routes[k : k + 1, :] == ids
        member += jnp.where(hit, 1.0, 0.0)
        row_weight += jnp.where(hit, route_weights[k : k + 1, :], 0.0)
    before = lax.broadcasted_iota(jnp.int32, (tok_rows, tok_rows), 0) < lax.broadcasted_iota(
        jnp.int32, (tok_rows, tok_rows), 1
    )
    counts = jnp.dot(member.astype(bf16), before.astype(bf16), preferred_element_type=f32)
    position = jnp.where(member > 0.0, counts, -1.0)
    meta[...] = jnp.zeros(meta.shape, f32)
    for e in range(n):
        meta[e, 0:1, :] = position[e : e + 1, :]
        meta[e, 1:2, :] = row_weight[e : e + 1, :]
    metas[me] = meta[me]

    pl.semaphore_wait(barrier, n + groups - 2)

    meta_copies = []
    for k in range(1, n):
        peer = lax.rem(me + k, n)
        meta_copies.append(
            push(meta.at[peer], metas.at[me], meta_send.at[k], meta_recv.at[k], (peer, tp))
        )

    spots = iter(range(token_send.shape[0]))

    def push_tokens(block, device_z, device_x, keep=True):
        spot = next(spots)
        return push(
            gathered.at[block],
            gathered.at[block],
            token_send.at[spot],
            token_recv.at[block],
            (at(device_z, device_x), tp),
            keep,
        )

    push_tokens(me, far_way, x)
    for i in range(1, span):
        push_tokens(me, near(i), x)
    for dx in range(1, nx):
        push_tokens(me, z, beside(dx))

    def push_weights(j, q):
        push(
            staged.at[j, q],
            readies[j].at[rows_of(me)],
            weight_send.at[j, q],
            weight_recv.at[j, me],
            (places[q], tp),
        )

    def convert(i):
        j, q = blocks[i]
        fetches[i].wait()
        value = wide[i % DEPTH]
        if j < 2:
            value = gain[...] * value
        if q == n - 1:
            readies[j][rows_of(me), :] = value.astype(bf16)
        else:
            staged[j, q] = value.astype(bf16)
        if i + DEPTH < len(blocks):
            fetches.append(fetch(i + DEPTH))

    for q in range(n):
        convert(q)
        if q > 0:
            push_weights(0, q - 1)
    for q in range(n):
        convert(n + q)

    for copy in meta_copies:
        copy.wait_recv()

    def await_tokens(block):
        remote(
            gathered.at[block],
            gathered.at[block],
            token_send.at[0],
            token_recv.at[block],
            (me, partner),
        ).wait_recv()

    def share_block(block):
        def to(step, device):
            remote(
                routed.at[tp, slots_of(block)],
                routed.at[tp, slots_of(block)],
                share_send.at[step],
                share_recv.at[step],
                (me, device),
            ).start()

        for h in range(1, chips):
            to(h, lax.rem(chip + h, chips) * CORES + core)
        to(0, partner)

    lines = lax.broadcasted_iota(jnp.int32, (capacity, tok_rows), 0).astype(f32)
    columns_of = lax.broadcasted_iota(jnp.int32, (tok_rows, capacity), 1).astype(f32)
    diagonal = lax.broadcasted_iota(jnp.int32, (tok_rows, tok_rows), 0) == lax.broadcasted_iota(
        jnp.int32, (tok_rows, tok_rows), 1
    )
    pending = []

    def pick(block):
        place = metas[block, 0:1, :]
        weight = metas[block, 1:2, :]
        chosen = jnp.where(place == lines, 1.0, 0.0).astype(bf16)
        routed[tp, slots_of(block), :] = jnp.dot(
            chosen, gathered[block], preferred_element_type=f32
        ).astype(bf16)
        if pending:
            share_block(pending.pop())
        ones = jnp.ones((tok_rows, capacity), bf16)
        place_down = jnp.dot(
            jnp.where(diagonal, place, 0.0).astype(bf16), ones, preferred_element_type=f32
        )
        weight_down = jnp.dot(
            jnp.where(diagonal, weight, 0.0).astype(bf16), ones, preferred_element_type=f32
        )
        tables[block] = jnp.where(place_down == columns_of, weight_down, 0.0).astype(bf16)
        pending.append(block)

    relays = []
    column = [near(i) for i in range(span)] + [far(i) for i in range(span)]
    for i in range(nz + 1):
        if i < nz:
            block = at(column[i], x)
            if i > 0:
                await_tokens(block)
                if i >= span:
                    spot = [next(spots) for _ in range(1, span)]

                    @pl.when(z == gate_way)
                    def _(block=block, spot=spot):
                        for m in range(1, span):
                            remote(
                                gathered.at[block],
                                gathered.at[block],
                                token_send.at[spot[m - 1]],
                                token_recv.at[block],
                                (at(near(m), x), tp),
                            ).start()

                    relays += [(block, spot[m - 1], near(m)) for m in range(1, span)]
                for dx in range(1, nx):
                    push_tokens(block, z, beside(dx))
        if i > 0:
            for dx in range(1, nx):
                other = at(column[i - 1], beside(dx))
                await_tokens(other)
                pick(other)
        if i < nz:
            pick(block)
    share_block(pending.pop())

    for q in range(n - 1):
        push_weights(1, q)
    for q in range(n):
        convert(2 * n + q)

    def all_rows(step, origin, device):
        return remote(
            routed.at[tp], routed.at[origin], share_send.at[step], share_recv.at[step], (me, device)
        )

    shared = []
    for h in range(1, chips):
        origin = lax.rem(chip - h + chips, chips) * CORES + core
        copy = all_rows(h, origin, partner)
        copy.wait_recv()
        shared.append(copy)
        push(
            routed.at[origin],
            routed.at[origin],
            forward_send.at[h],
            forward_recv.at[h],
            (me, partner),
        )
    copy = all_rows(0, partner, partner)
    copy.wait_recv()
    shared.append(copy)
    for h in range(1, chips):
        origin = lax.rem(chip - h + chips, chips) * CORES + (CORES - 1 - core)
        remote(
            routed.at[origin],
            routed.at[origin],
            forward_send.at[h],
            forward_recv.at[h],
            (me, partner),
        ).wait_recv()

    def await_weights(j):
        for k in range(1, n):
            source = lax.rem(me + k, n)
            remote(
                staged.at[j, 0],
                readies[j].at[rows_of(source)],
                weight_send.at[j, 0],
                weight_recv.at[j, source],
                (me, partner),
            ).wait_recv()

    def product(rows, ready):
        total = jnp.zeros((row_tile, hidden.shape[1]), f32)
        for t in range(groups):
            total += jnp.dot(
                routed[t, rows, :],
                ready[t * part : (t + 1) * part],
                preferred_element_type=f32,
            )
        return total

    def tiles(body):
        @pl.loop(0, total_slots // row_tile)
        def _(tile):
            body(pl.ds(pl.multiple_of(tile * row_tile, 16), row_tile))

    await_weights(0)

    @tiles
    def _(rows):
        gate_pre[rows, :] = product(rows, gate_ready)

    def push_down(i):
        for q in range(n - 1):
            push(
                staged.at[2, q, pl.ds(i * piece, piece)],
                down_ready.at[chunk_of(me, i)],
                down_send.at[i, q],
                down_recv.at[i, me],
                (places[q], tp),
            )

    for i in range(min(2, chunks)):
        push_down(i)

    await_weights(1)

    @tiles
    def _(rows):
        hidden[rows, :] = activate(gate_pre[rows, :], product(rows, up_ready)).astype(bf16)

    over_copies = {}

    def project(i):
        for k in range(1, n):
            source = lax.rem(me + k, n)
            remote(
                staged.at[2, 0, pl.ds(0, piece)],
                down_ready.at[chunk_of(source, i)],
                down_send.at[i, 0],
                down_recv.at[i, source],
                (me, partner),
            ).wait_recv()

        def run(side, target):
            picked = [
                down_ready[
                    chunk_of((lax.rem(chip + h, chips) * CORES + side) * shares + r, i), :
                ]
                for h in range(chips)
                for r in range(shares)
            ]
            down = jnp.concatenate(picked, axis=0)

            @tiles
            def _(rows):
                value = lax.dot_general(
                    hidden[rows, :], down, (((1,), (1,)), ((), ())), preferred_element_type=f32
                ).astype(bf16)
                for h in range(chips):
                    target[i, h, rows, :] = value[:, h * LANES : (h + 1) * LANES]

        run(CORES - 1 - core, given)
        pair = push(
            given.at[i], partner_sums.at[i], pair_send.at[i], pair_recv.at[i], (me, partner)
        )
        run(core, kept)
        pair.wait_recv()
        for h in range(1, chips):

            @tiles
            def _(rows, h=h):
                total = kept[i, h, rows, :].astype(f32) + partner_sums[i, h, rows, :].astype(f32)
                kept[i, h, rows, :] = total.astype(bf16)

            over_copies[i, h] = push(
                kept.at[i, h],
                chip_sums.at[i, h - 1],
                chip_send.at[i, h],
                chip_recv.at[i, h],
                (me, lax.rem(chip + h, chips) * CORES + core),
            )

    x_copies = {}

    def combine(i):
        for h in range(1, chips):
            over_copies[i, h].wait_recv()

        @tiles
        def _(rows):
            total = kept[i, 0, rows, :].astype(f32) + partner_sums[i, 0, rows, :].astype(f32)
            for h in range(1, chips):
                total += chip_sums[i, h - 1, rows, :].astype(f32)
            expert_out[rows, :] = total.astype(bf16)

        def rows_for(block):
            return jnp.dot(
                tables[block], expert_out[slots_of(block), :], preferred_element_type=f32
            )

        for dx in range(1, nx):
            for zz in range(nz):
                x_out[i, dx - 1, zz] = rows_for(at(zz, beside(dx))).astype(bf16)
            x_copies[i, dx] = push(
                x_out.at[i, dx - 1],
                x_in.at[i, dx - 1],
                x_send.at[i, dx],
                x_recv.at[i, dx],
                (at(z, beside(dx)), tp),
            )
        for zz in range(nz):
            row_sums[i, zz] = rows_for(at(zz, x))

    near_copies = {}

    def far_copy(i, device_z, slot):
        return remote(
            far_out.at[i],
            far_in.at[i, slot],
            far_send.at[i],
            far_recv.at[i, slot],
            (at(device_z, x), tp),
        )

    def spread(i):
        for dx in range(1, nx):
            x_copies[i, dx].wait_recv()
        for zz in range(nz):
            total = row_sums[i, zz]
            for dx in range(1, nx):
                total += x_in[i, dx - 1, zz].astype(f32)
            row_sums[i, zz] = total

        @pl.when(z != gate_way)
        def _():
            for f in range(span):
                far_out[i, f] = row_sums[i, (1 - half) * span + f].astype(bf16)
            far_copy(i, gate_way, local).start()

        for m in range(1, span):
            near_out[i, m - 1] = row_sums[i, near(m)].astype(bf16)
            near_copies[i, m] = push(
                near_out.at[i, m - 1],
                near_in.at[i, m - 1],
                near_send.at[i, m],
                near_recv.at[i, m],
                (at(near(m), x), tp),
            )

    def cross_copy(i, f):
        return remote(
            cross_out.at[i, f],
            cross_in.at[i],
            cross_send.at[i, f],
            cross_recv.at[i],
            (at((1 - half) * span + f, x), tp),
        )

    def cross(i):
        @pl.when(z == gate_way)
        def _():
            for m in range(1, span):
                far_copy(i, near(m), lax.rem(local + m, span)).wait_recv()
            for f in range(span):
                total = row_sums[i, (1 - half) * span + f]
                for m in range(1, span):
                    total += far_in[i, lax.rem(local + m, span), f].astype(f32)
                cross_out[i, f] = total.astype(bf16)
                cross_copy(i, f).start()

    def finish(i):
        total = row_sums[i, z]
        for m in range(1, span):
            near_copies[i, m].wait_recv()
            total += near_in[i, m - 1].astype(f32)
        cross_copy(i, 0).wait_recv()
        total += cross_in[i].astype(f32)
        finished[:, i * LANES : (i + 1) * LANES] = total.astype(bf16)

    stages = (finish, cross, spread, combine)
    for step in range(chunks + len(stages)):
        for late, stage in enumerate(stages):
            i = step - (len(stages) - late)
            if 0 <= i < chunks:
                stage(i)
        if step < chunks:
            if step + 2 < chunks:
                push_down(step + 2)
            project(step)

    column_to = lax.broadcasted_iota(jnp.int32, (part, part), 1)
    share_to = column_to // source_rows
    inner_to = lax.rem(column_to, source_rows)
    from_to = (inner_to // piece) * LANES + share_to * piece + lax.rem(inner_to, piece)
    order = (lax.broadcasted_iota(jnp.int32, (part, part), 0) == from_to).astype(bf16)
    out[...] = jnp.dot(finished[...], order, preferred_element_type=f32).astype(bf16)

    @pl.when(z == gate_way)
    def _():
        for block, spot, device_z in relays:
            remote(
                gathered.at[block],
                gathered.at[block],
                token_send.at[spot],
                token_recv.at[block],
                (at(device_z, x), tp),
            ).wait_send()
        for i in range(chunks):
            for f in range(span):
                cross_copy(i, f).wait_send()

    @pl.when(z != gate_way)
    def _():
        for i in range(chunks):
            far_copy(i, gate_way, local).wait_send()

    for copy in sends + shared:
        copy.wait_send()


def hand_over(tokens, gain, routes, route_weights, gate_local, up_local, down_local):
    n = lax.axis_size("fs")
    groups = lax.axis_size("tp")
    tok_rows, width = tokens.shape
    top_count = routes.shape[0]
    source_rows, units = gate_local.shape[1:]
    capacity = 3 * tok_rows * top_count // (2 * n)
    total_slots = n * capacity
    part = width // groups
    chips = groups // CORES
    nx = line_width(n)
    nz = n // nx
    span = nz // 2
    chunks = part // LANES
    vmem = pl.BlockSpec(memory_space=pltpu.VMEM)
    anywhere = pl.BlockSpec(memory_space=pl.ANY)
    bf16, f32 = jnp.bfloat16, jnp.float32
    ready = jax.ShapeDtypeStruct((width, units), bf16)
    dma = pltpu.SemaphoreType.DMA
    token_sends = 1 + (span - 1) + nz * (nx - 1) + span * (span - 1)
    rows = (tok_rows, LANES)
    return pl.pallas_call(
        functools.partial(kernel, n, groups, nx, total_slots // 4),
        out_shape=(ready, ready, ready, jax.ShapeDtypeStruct((tok_rows, part), bf16)),
        in_specs=[anywhere] + [vmem] * 3 + [anywhere] * 3,
        out_specs=(vmem,) * 4,
        scratch_shapes=[
            pltpu.VMEM((DEPTH, source_rows, units), f32),
            pltpu.VMEM((tok_rows, width), bf16),
            pltpu.VMEM((3, n - 1, source_rows, units), bf16),
            pltpu.VMEM((n, tok_rows, part), bf16),
            pltpu.VMEM((n, 8, tok_rows), f32),
            pltpu.VMEM((n, 8, tok_rows), f32),
            pltpu.VMEM((n, tok_rows, capacity), bf16),
            pltpu.VMEM((groups, total_slots, part), bf16),
            pltpu.VMEM((total_slots, units), f32),
            pltpu.VMEM((total_slots, units), bf16),
            pltpu.VMEM((chunks, chips, total_slots, LANES), bf16),
            pltpu.VMEM((chunks, chips, total_slots, LANES), bf16),
            pltpu.VMEM((chunks, chips, total_slots, LANES), bf16),
            pltpu.VMEM((chunks, chips - 1, total_slots, LANES), bf16),
            pltpu.VMEM((total_slots, LANES), bf16),
            pltpu.VMEM((chunks, nz) + rows, f32),
            pltpu.VMEM((chunks, nx - 1, nz) + rows, bf16),
            pltpu.VMEM((chunks, nx - 1, nz) + rows, bf16),
            pltpu.VMEM((chunks, span) + rows, bf16),
            pltpu.VMEM((chunks, span) + rows, bf16),
            pltpu.VMEM((chunks, span) + rows, bf16),
            pltpu.VMEM((chunks, span, span) + rows, bf16),
            pltpu.VMEM((chunks, span) + rows, bf16),
            pltpu.VMEM((chunks,) + rows, bf16),
            pltpu.VMEM((tok_rows, part), bf16),
            dma((DEPTH,)),
            dma,
            dma((n,)),
            dma((n,)),
            dma((token_sends,)),
            dma((n,)),
            dma((chips,)),
            dma((chips,)),
            dma((chips,)),
            dma((chips,)),
            dma((2, n)),
            dma((2, n)),
            dma((chunks, n)),
            dma((chunks, n)),
            dma((chunks,)),
            dma((chunks,)),
            dma((chunks, chips)),
            dma((chunks, chips)),
            dma((chunks, nx)),
            dma((chunks, nx)),
            dma((chunks, span)),
            dma((chunks, span)),
            dma((chunks,)),
            dma((chunks, span)),
            dma((chunks, span)),
            dma((chunks,)),
        ],
        compiler_params=pltpu.CompilerParams(
            collective_id=0, has_side_effects=True, vmem_limit_bytes=58 * 1024 * 1024
        ),
    )(tokens, gain, routes, route_weights, gate_local, up_local, down_local)


def body(tokens, norm_gain, gate_weight, up_weight, down_weight, routes, route_weights):
    gate_ready, up_ready, down_ready, moe_output = hand_over(
        tokens,
        norm_gain[:, None],
        routes.T,
        route_weights.T.astype(jnp.float32),
        gate_weight,
        up_weight,
        down_weight,
    )
    return (gate_ready[None], up_ready[None], down_ready[None], moe_output)


def solution(mesh):
    in_specs = (
        P("fs", None),
        P("fs"),
        P(None, "fs", "tp"),
        P(None, "fs", "tp"),
        P(None, "fs", "tp"),
        P("fs", None),
        P("fs", None),
    )
    out_specs = (P("fs", None, "tp"), P("fs", None, "tp"), P("fs", None, "tp"), P("fs", "tp"))
    return jax.shard_map(body, mesh=mesh, in_specs=in_specs, out_specs=out_specs, check_vma=False)
```

time: 247 us -> 222 us (0.90)
  the two profiles are of different devices: /device:TPU:19 before, /device:TPU:0 now
where the time goes in v1:
time: 222 us
  Pallas kernels  211 us (95%)
  local copies, waits for them, and re-layouts  9.04 us (4%)
    pallas_call x1, Pallas kernels, hand_over(): pl.pallas_call(functools.partial(kernel, n, groups, nx, total_slots // 4)...  211 us
    unnamed x10, local copies, waits for them, and re-layouts  7.57 us

profile of v1, /device:TPU:0, one launch (start us, length us, event | category | flops | bytes accessed | tf_op | source)
XLA Modules:
  0.0 221.7 jit_solution(14375269985481602345)
XLA Ops:
  0.6 1.3 convert_bitcast_fusion.route_weights
  1.9 1.5 copy.11.gain
  3.4 210.7 %shard_map.102 = (bf16[2048,512]{1,0:T(8,128)(2,1)}, bf16[2048,512]{1,0:T(8,128)(2,1)}, bf16[2048,512]{1,0:T(8,128)(2,1)}, bf16[256,512]{1,0:T(8,128)(2,1)}) custom-call(bf16[256,2048]{1,0:T(8,128)(2,1)} %tokens.1, f32[256,1]{1,0:T(8,128)} %copy.11.gain, s32[4,256]{1,0:T(4,128)} %bitcast.10, f32[4,256]{1,0:T(4,128)} %convert_bitcast_fusion.route_weights, ...), custom_call_target="tpu_custom_call" | custom-call | tf_op jit(solution)/shard_map/pallas_call | solution.py:661
  214.1 0.0 copy-start.1
  214.1 3.2 %copy.16 = bf16[1,2048,512]{2,1,0:T(8,128)(2,1)} copy(bf16[1,2048,512]{2,1,0:T(8,128)(2,1)} %bitcast.9) | data formatting | bytes 4194304
  217.3 0.0 copy-done.1
  217.3 0.0 copy-start
  217.3 1.3 copy.17
  218.7 1.0 copy-done
  219.7 0.0 copy-start.2
  219.7 1.3 copy.18
  221.0 0.0 copy-done.2
  221.0 0.7 copy.19
Async XLA Ops:
  214.1 3.2 %copy-start.1 = (bf16[2048,512]{1,0:T(8,128)(2,1)S(1)}, bf16[2048,512]{1,0:T(8,128)(2,1)}, u32[]{:S(2)}) copy-start(bf16[2048,512]{1,0:T(8,128)(2,1)} %get-tuple-element.9) | copy-start | bytes 6291460
  217.3 2.3 %copy-start = (bf16[2048,512]{1,0:T(8,128)(2,1)S(1)}, bf16[2048,512]{1,0:T(8,128)(2,1)}, u32[]{:S(2)}) copy-start(bf16[2048,512]{1,0:T(8,128)(2,1)} %get-tuple-element.10) | copy-start | bytes 6291460
  219.7 1.3 copy-start.2

commit v2 on v1

v2 whole, which is shorter than its diff:
```python
import functools

import jax
import jax.numpy as jnp
from jax import lax
from jax.experimental import pallas as pl
from jax.experimental.pallas import tpu as pltpu
from jax.sharding import PartitionSpec as P

norm_eps = 1e-06
clamp_limit = 7.0
gate_alpha = 1.702
MESH = pl.DeviceIdType.MESH
CORES = 2
DEPTH = 6
LANES = 128


def activate(gate_pre, up_pre):
    gate_part = jnp.minimum(gate_pre, clamp_limit)
    up_part = jnp.clip(up_pre, -clamp_limit, clamp_limit)
    return (up_part + 1.0) * gate_part * jax.nn.sigmoid(gate_alpha * gate_part)


def line_width(n):
    width = 1
    while 4 * width * width <= n:
        width *= 2
    return width


def kernel(
    n,
    groups,
    nx,
    row_tile,
    tokens,
    gain_in,
    routes_in,
    route_weights_in,
    gate_local,
    up_local,
    down_local,
    gate_ready,
    up_ready,
    down_ready,
    out,
    wide,
    token_rows,
    gain_row,
    gain,
    scale,
    routes,
    route_weights,
    staged,
    gathered,
    meta,
    metas,
    tables,
    routed,
    gate_pre,
    hidden,
    given,
    kept,
    partner_sums,
    chip_sums,
    expert_out,
    row_sums,
    x_out,
    x_in,
    near_out,
    near_in,
    far_out,
    far_in,
    cross_out,
    cross_in,
    finished,
    wide_sem,
    input_sem,
    meta_send,
    meta_recv,
    token_send,
    relay_send,
    token_recv,
    share_send,
    share_recv,
    forward_send,
    forward_recv,
    weight_send,
    weight_recv,
    down_recv,
    pair_send,
    pair_recv,
    chip_send,
    chip_recv,
    x_send,
    x_recv,
    near_send,
    near_recv,
    far_send,
    far_recv,
    cross_send,
    cross_recv,
):
    me = lax.axis_index("fs")
    tp = lax.axis_index("tp")
    chips = groups // CORES
    chip = tp // CORES
    core = lax.rem(tp, CORES)
    partner = chip * CORES + (CORES - 1 - core)
    nz = n // nx
    span = nz // 2
    z = me // nx
    x = lax.rem(me, nx)
    half = z // span
    local = lax.rem(z, span)
    gate_way = span - 1 + half
    far_way = span - half
    tok_rows, width = token_rows.shape
    part = width // groups
    source_rows = gate_local.shape[1]
    shares = n // groups
    total_slots = hidden.shape[0]
    capacity = total_slots // n
    chunks = given.shape[0]
    piece = source_rows // chunks
    f32, bf16 = jnp.float32, jnp.bfloat16

    def at(zz, xx):
        return zz * nx + xx

    def near(i):
        return half * span + lax.rem(local + i, span)

    def far(i):
        return (1 - half) * span + lax.rem(local + i, span)

    def beside(dx):
        return lax.rem(x + dx, nx)

    def slots_of(block):
        return pl.ds(pl.multiple_of(block * capacity, 16), capacity)

    def rows_of(block):
        return pl.ds(pl.multiple_of(block * source_rows, 16), source_rows)

    def chunk_of(block, i):
        return pl.ds(pl.multiple_of(block * source_rows + i * piece, 16), piece)

    group_rows = nx * capacity
    lane_rows = tok_rows // LANES

    def remote(src, dst, send_sem, recv_sem, device):
        return pltpu.make_async_remote_copy(
            src_ref=src,
            dst_ref=dst,
            send_sem=send_sem,
            recv_sem=recv_sem,
            device_id=device,
            device_id_type=MESH,
        )

    def push(src, dst, send_sem, recv_sem, device):
        copy = remote(src, dst, send_sem, recv_sem, device)
        copy.start()
        return copy

    def bulk(ref, send_sem, recv_sem):
        return remote(ref, ref, send_sem, recv_sem, (me, partner))

    peers = [at(far(i), beside(dx)) for dx in range(nx) for i in range(span)]
    peers += [at(near(i), beside(dx)) for dx in range(nx) for i in range(span) if i + dx > 0]
    places = peers + [me]
    locals_ = (gate_local, up_local, down_local)
    readies = (gate_ready, up_ready, down_ready)
    blocks = [(j, q) for j in range(3) for q in range(n)]

    def fetch(i):
        j, q = blocks[i]
        copy = pltpu.make_async_copy(
            locals_[j].at[places[q]], wide.at[i % DEPTH], wide_sem.at[i % DEPTH]
        )
        copy.start()
        return copy

    inputs = [
        pltpu.make_async_copy(src, dst, input_sem.at[spot])
        for spot, (src, dst) in enumerate(
            (
                (gain_in, gain_row),
                (tokens, token_rows),
                (routes_in, routes),
                (route_weights_in, route_weights),
            )
        )
    ]
    own_columns = pl.ds(pl.multiple_of(tp * part, LANES), part)
    inputs.append(
        pltpu.make_async_copy(tokens.at[:, own_columns], gathered.at[me], input_sem.at[4])
    )
    for copy in inputs:
        copy.start()
    fetches = [fetch(i) for i in range(DEPTH)]

    barrier = pltpu.get_barrier_semaphore()
    for k in range(1, n):
        pl.semaphore_signal(
            barrier, inc=1, device_id=(lax.rem(me + k, n), tp), device_id_type=MESH
        )
    for k in range(1, groups):
        pl.semaphore_signal(
            barrier, inc=1, device_id=(me, lax.rem(tp + k, groups)), device_id_type=MESH
        )

    inputs[0].wait()
    gain_at = lax.broadcasted_iota(jnp.int32, (source_rows, source_rows), 0) == (
        lax.broadcasted_iota(jnp.int32, (source_rows, source_rows), 1)
    )
    gain[...] = jnp.sum(jnp.where(gain_at, gain_row[...], 0.0), axis=1, keepdims=True)

    def push_weights(j, q):
        push(
            staged.at[j, q],
            readies[j].at[rows_of(me)],
            weight_send,
            weight_recv.at[j],
            (places[q], tp),
        )

    def convert(i):
        j, q = blocks[i]
        fetches[i].wait()
        value = wide[i % DEPTH]
        if j < 2:
            value = gain[...] * value
        if q == n - 1:
            readies[j][rows_of(me), :] = value.astype(bf16)
        else:
            staged[j, q] = value.astype(bf16)
        if i + DEPTH < len(blocks):
            fetches.append(fetch(i + DEPTH))

    pl.semaphore_wait(barrier, n + groups - 2)

    def push_tokens(block, device_z, device_x):
        push(
            tokens.at[:, own_columns],
            gathered.at[block],
            token_send,
            token_recv.at[block],
            (at(device_z, device_x), tp),
        )

    beside_half = [(i, dx) for dx in range(nx) for i in range(span) if i + dx > 0]
    push_tokens(me, far_way, x)
    for i, dx in beside_half:
        push_tokens(me, near(i), beside(dx))
    convert(0)
    for copy in inputs[1:]:
        copy.wait()

    @pl.loop(0, tok_rows // 32)
    def _(tile):
        rows = pl.ds(pl.multiple_of(tile * 32, 32), 32)
        wide_rows = token_rows[rows, :].astype(f32)
        scale[rows, :] = lax.rsqrt(
            jnp.mean(wide_rows * wide_rows, axis=1, keepdims=True) + norm_eps
        )

    ids = lax.broadcasted_iota(jnp.int32, (n, tok_rows), 0)
    member = jnp.zeros((n, tok_rows), f32)
    row_weight = jnp.zeros((n, tok_rows), f32)
    given_weights = route_weights[...].astype(f32)
    for k in range(routes.shape[0]):
        hit = routes[k : k + 1, :] == ids
        member += jnp.where(hit, 1.0, 0.0)
        row_weight += jnp.where(hit, given_weights[k : k + 1, :], 0.0)
    down_index = lax.broadcasted_iota(jnp.int32, (tok_rows, tok_rows), 0)
    across_index = lax.broadcasted_iota(jnp.int32, (tok_rows, tok_rows), 1)
    before = down_index < across_index
    diagonal = down_index == across_index
    scale_row = jnp.sum(jnp.where(diagonal, scale[...], 0.0), axis=0, keepdims=True)
    counts = jnp.dot(member.astype(bf16), before.astype(bf16), preferred_element_type=f32)
    position = jnp.where(member > 0.0, counts, -1.0)
    meta[...] = jnp.zeros(meta.shape, f32)
    for e in range(n):
        for r in range(lane_rows):
            lanes = slice(r * LANES, (r + 1) * LANES)
            meta[e, r : r + 1, :] = position[e : e + 1, lanes]
            meta[e, lane_rows + r : lane_rows + r + 1, :] = row_weight[e : e + 1, lanes]
            meta[e, 2 * lane_rows + r : 2 * lane_rows + r + 1, :] = scale_row[:, lanes]
    metas[me] = meta[me]

    for k in range(1, n):
        peer = lax.rem(me + k, n)
        push(meta.at[peer], metas.at[me], meta_send, meta_recv, (peer, tp))

    for q in range(1, n):
        convert(q)
        if q <= span:
            push_weights(0, q - 1)
    for q in range(n):
        convert(n + q)

    def push_rest():
        for q in range(span, n - 1):
            push_weights(0, q)

    def push_up():
        for q in range(n - 1):
            push_weights(1, q)

    @pl.when(z != gate_way)
    def _():
        push_rest()
        push_up()

    bulk(metas.at[pl.ds(0, n - 1)], meta_send, meta_recv).wait_recv()

    def await_tokens(block):
        bulk(gathered.at[block], token_send, token_recv.at[block]).wait_recv()

    def share_block(block):
        def to(step, device):
            remote(
                routed.at[tp, slots_of(block)],
                routed.at[tp, slots_of(block)],
                share_send.at[step],
                share_recv.at[step],
                (me, device),
            ).start()

        for h in range(1, chips):
            to(h, lax.rem(chip + h, chips) * CORES + core)
        to(0, partner)

    lines = lax.broadcasted_iota(jnp.int32, (capacity, tok_rows), 0).astype(f32)
    columns_of = lax.broadcasted_iota(jnp.int32, (tok_rows, capacity), 1).astype(f32)
    pending = []

    def pick(block):
        found = metas[block]
        place, weight, scale_across = (
            jnp.concatenate([found[j + r : j + r + 1, :] for r in range(lane_rows)], axis=1)
            for j in (0, lane_rows, 2 * lane_rows)
        )
        chosen = jnp.where(place == lines, 1.0, 0.0).astype(bf16)
        scale_down = jnp.sum(jnp.where(diagonal, scale_across, 0.0), axis=1, keepdims=True)
        normed = (gathered[block].astype(f32) * scale_down).astype(bf16)
        routed[tp, slots_of(block), :] = jnp.dot(
            chosen, normed, preferred_element_type=f32
        ).astype(bf16)
        if pending:
            share_block(pending.pop())
        ones = jnp.ones((tok_rows, capacity), bf16)
        place_down = jnp.dot(
            jnp.where(diagonal, place, 0.0).astype(bf16), ones, preferred_element_type=f32
        )
        weight_down = jnp.dot(
            jnp.where(diagonal, weight, 0.0).astype(bf16), ones, preferred_element_type=f32
        )
        tables[block] = jnp.where(place_down == columns_of, weight_down, 0.0).astype(bf16)
        pending.append(block)

    pick(me)
    for i, dx in beside_half:
        block = at(near(i), beside(dx))
        await_tokens(block)
        pick(block)
    for i in range(span):
        block = at(far(i), x)
        await_tokens(block)

        @pl.when(z == gate_way)
        def _(i=i, block=block):
            for m, dx in beside_half:
                push(
                    gathered.at[block],
                    gathered.at[block],
                    relay_send.at[i],
                    token_recv.at[block],
                    (at(near(m), beside(dx)), tp),
                )

    pl.when(z == gate_way)(push_rest)
    for dx in range(nx):
        for i in range(span):
            block = at(far(i), beside(dx))
            if dx > 0:
                await_tokens(block)
            pick(block)
    share_block(pending.pop())

    pl.when(z == gate_way)(push_up)
    for q in range(n):
        convert(2 * n + q)

    def all_rows(step, origin, device):
        return remote(
            routed.at[tp], routed.at[origin], share_send.at[step], share_recv.at[step], (me, device)
        )

    shared = []
    for h in range(1, chips):
        origin = lax.rem(chip - h + chips, chips) * CORES + core
        copy = all_rows(h, origin, partner)
        copy.wait_recv()
        shared.append(copy)
        push(
            routed.at[origin],
            routed.at[origin],
            forward_send.at[h],
            forward_recv.at[h],
            (me, partner),
        )
    copy = all_rows(0, partner, partner)
    copy.wait_recv()
    shared.append(copy)
    for h in range(1, chips):
        origin = lax.rem(chip - h + chips, chips) * CORES + (CORES - 1 - core)
        remote(
            routed.at[origin],
            routed.at[origin],
            forward_send.at[h],
            forward_recv.at[h],
            (me, partner),
        ).wait_recv()

    def await_weights(j):
        received = readies[j].at[pl.ds(0, (n - 1) * source_rows)]
        bulk(received, weight_send, weight_recv.at[j]).wait_recv()

    def product(rows, ready):
        total = jnp.zeros((row_tile, hidden.shape[1]), f32)
        for t in range(groups):
            total += jnp.dot(
                routed[t, rows, :],
                ready[t * part : (t + 1) * part],
                preferred_element_type=f32,
            )
        return total

    def tiles(body):
        @pl.loop(0, total_slots // row_tile)
        def _(tile):
            body(pl.ds(pl.multiple_of(tile * row_tile, 16), row_tile))

    await_weights(0)

    @tiles
    def _(rows):
        gate_pre[rows, :] = product(rows, gate_ready)

    def push_down(i):
        for q in range(n - 1):
            push(
                staged.at[2, q, pl.ds(i * piece, piece)],
                down_ready.at[chunk_of(me, i)],
                weight_send,
                down_recv.at[i],
                (places[q], tp),
            )

    @pl.when(z == gate_way)
    def _():
        for i in range(chunks):
            push_down(i)

    await_weights(1)
    pl.when(z != gate_way)(functools.partial(push_down, 0))

    @tiles
    def _(rows):
        hidden[rows, :] = activate(gate_pre[rows, :], product(rows, up_ready)).astype(bf16)

    over_copies = {}
    units = [(1 - half) * span + f for f in range(span)]
    units += [near(m) for m in range(1, span)] + [z]
    mates = range(span, nz - 1)
    own_unit = nz - 1

    def rows_in(u):
        return pl.ds(pl.multiple_of(units[u] * group_rows, 16), group_rows)

    def project(i):
        received = down_ready.at[pl.ds(0, (n - 1) * piece)]
        bulk(received, weight_send, down_recv.at[i]).wait_recv()
        if i + 1 < chunks:
            pl.when(z != gate_way)(functools.partial(push_down, i + 1))

        def rows_to(side):
            picked = [
                down_ready[
                    chunk_of((lax.rem(chip + h, chips) * CORES + side) * shares + r, i), :
                ]
                for h in range(chips)
                for r in range(shares)
            ]
            return jnp.concatenate(picked, axis=0)

        def run(down, target, u):
            rows = rows_in(u)
            value = lax.dot_general(
                hidden[rows, :], down, (((1,), (1,)), ((), ())), preferred_element_type=f32
            ).astype(bf16)
            for h in range(chips):
                target[i, h, rows, :] = value[:, h * LANES : (h + 1) * LANES]

        give = rows_to(CORES - 1 - core)
        for u in range(nz):
            run(give, given, u)
            for h in range(chips):
                push(
                    given.at[i, h, rows_in(u)],
                    partner_sums.at[i, h, rows_in(u)],
                    pair_send,
                    pair_recv.at[i, u],
                    (me, partner),
                )
        keep = rows_to(core)
        for u in range(nz):
            rows = rows_in(u)
            run(keep, kept, u)
            bulk(given.at[i, pl.ds(0, chips), rows], pair_send, pair_recv.at[i, u]).wait_recv()
            for h in range(1, chips):
                total = kept[i, h, rows, :].astype(f32)
                total += partner_sums[i, h, rows, :].astype(f32)
                kept[i, h, rows, :] = total.astype(bf16)
                over_copies[i, h, u] = push(
                    kept.at[i, h, rows],
                    chip_sums.at[i, h - 1, rows],
                    chip_send,
                    chip_recv.at[i, h, u],
                    (me, lax.rem(chip + h, chips) * CORES + core),
                )

    x_copies = {}

    def combine(i, u):
        for h in range(1, chips):
            over_copies[i, h, u].wait_recv()

        rows = rows_in(u)
        total = kept[i, 0, rows, :].astype(f32) + partner_sums[i, 0, rows, :].astype(f32)
        for h in range(1, chips):
            total += chip_sums[i, h - 1, rows, :].astype(f32)
        expert_out[rows, :] = total.astype(bf16)

        def rows_for(xx):
            block = at(units[u], xx)
            return jnp.dot(
                tables[block], expert_out[slots_of(block), :], preferred_element_type=f32
            )

        for dx in range(1, nx):
            x_out[i, dx - 1, u] = rows_for(beside(dx)).astype(bf16)
            x_copies[i, dx, u] = push(
                x_out.at[i, dx - 1, u],
                x_in.at[i, dx - 1, u],
                x_send,
                x_recv.at[i, dx, u],
                (at(z, beside(dx)), tp),
            )
        row_sums[i, u] = rows_for(x)

    near_copies = {}

    def far_copy(i, u, device_z, slot):
        return remote(
            far_out.at[i, u],
            far_in.at[i, slot, u],
            far_send,
            far_recv.at[i, slot, u],
            (at(device_z, x), tp),
        )

    def spread(i, u):
        for dx in range(1, nx):
            x_copies[i, dx, u].wait_recv()
        total = row_sums[i, u]
        for dx in range(1, nx):
            total += x_in[i, dx - 1, u].astype(f32)
        row_sums[i, u] = total
        if u < span:

            @pl.when(z != gate_way)
            def _():
                far_out[i, u] = total.astype(bf16)
                far_copy(i, u, gate_way, local).start()

        elif u in mates:
            m = u - span + 1
            near_out[i, m - 1] = total.astype(bf16)
            near_copies[i, m] = push(
                near_out.at[i, m - 1],
                near_in.at[i, m - 1],
                near_send,
                near_recv.at[i, m - 1],
                (at(near(m), x), tp),
            )

    def cross(i, u):
        @pl.when(z == gate_way)
        def _():
            total = row_sums[i, u]
            for m in range(1, span):
                slot = lax.rem(local + m, span)
                far_copy(i, u, near(m), slot).wait_recv()
                total += far_in[i, slot, u].astype(f32)
            cross_out[i, u] = total.astype(bf16)
            push(
                cross_out.at[i, u],
                cross_in.at[i],
                cross_send,
                cross_recv.at[i],
                (at(units[u], x), tp),
            )

    def finish(i):
        total = row_sums[i, own_unit]
        for m in range(1, span):
            near_copies[i, m].wait_recv()
            total += near_in[i, m - 1].astype(f32)
        bulk(cross_in.at[i], cross_send, cross_recv.at[i]).wait_recv()
        total += cross_in[i].astype(f32)
        finished[:, i * LANES : (i + 1) * LANES] = total.astype(bf16)

    far_units, all_units = range(span), range(nz)

    def each(stage, i, which):
        if 0 <= i < chunks:
            for u in which:
                stage(i, u)

    for step in range(chunks):
        project(step)
        each(spread, step - 2, all_units)
        each(combine, step - 1, all_units)
    last = chunks - 1
    for u in all_units:
        combine(last, u)
        if last > 0:
            spread(last - 1, u)
        if u == span - 1:
            for i in range(last - 1):
                each(cross, i, far_units)
        if u >= span:
            spread(last, u - span)
    each(cross, last - 1, far_units)
    for u in range(nz - span, nz):
        cross(last, u - nz + span)
        spread(last, u)
    for i in range(chunks):
        finish(i)

    column_to = lax.broadcasted_iota(jnp.int32, (part, part), 1)
    share_to = column_to // source_rows
    inner_to = lax.rem(column_to, source_rows)
    from_to = (inner_to // piece) * LANES + share_to * piece + lax.rem(inner_to, piece)
    order = (lax.broadcasted_iota(jnp.int32, (part, part), 0) == from_to).astype(bf16)
    out[...] = jnp.dot(finished[...], order, preferred_element_type=f32).astype(bf16)

    @pl.when(z == gate_way)
    def _():
        for i in range(span):
            relayed = gathered.at[pl.ds(0, len(beside_half))]
            bulk(relayed, relay_send.at[i], meta_recv).wait_send()
        bulk(cross_out, cross_send, meta_recv).wait_send()

    @pl.when(z != gate_way)
    def _():
        bulk(far_out, far_send, meta_recv).wait_send()

    bulk(meta.at[pl.ds(0, n - 1)], meta_send, meta_recv).wait_send()
    bulk(gathered.at[pl.ds(0, len(beside_half) + 1)], token_send, meta_recv).wait_send()
    bulk(staged, weight_send, meta_recv).wait_send()
    bulk(given, pair_send, meta_recv).wait_send()
    bulk(chip_sums, chip_send, meta_recv).wait_send()
    bulk(x_out, x_send, meta_recv).wait_send()
    bulk(near_out, near_send, meta_recv).wait_send()
    for h in range(1, chips):
        bulk(routed.at[tp], forward_send.at[h], meta_recv).wait_send()
    for copy in shared:
        copy.wait_send()


def settle_kernel(*refs):
    count = (len(refs) - 1) // 2
    sems = refs[-1]
    copies = [
        pltpu.make_async_copy(refs[i], refs[count + i], sems.at[i]) for i in range(count)
    ]
    for copy in copies:
        copy.start()
    for copy in copies:
        copy.wait()


def settle(*arrays):
    anywhere = pl.BlockSpec(memory_space=pl.ANY)
    hbm = pl.BlockSpec(memory_space=pltpu.HBM)
    return pl.pallas_call(
        settle_kernel,
        out_shape=tuple(jax.ShapeDtypeStruct(a.shape, a.dtype) for a in arrays),
        in_specs=[anywhere] * len(arrays),
        out_specs=(hbm,) * len(arrays),
        scratch_shapes=[pltpu.SemaphoreType.DMA((len(arrays),))],
        compiler_params=pltpu.CompilerParams(vmem_limit_bytes=1024 * 1024),
    )(*arrays)


def hand_over(tokens, gain, routes, route_weights, gate_local, up_local, down_local):
    n = lax.axis_size("fs")
    groups = lax.axis_size("tp")
    tok_rows, width = tokens.shape
    top_count = routes.shape[0]
    source_rows, units = gate_local.shape[1:]
    capacity = 3 * tok_rows * top_count // (2 * n)
    total_slots = n * capacity
    part = width // groups
    chips = groups // CORES
    nx = line_width(n)
    nz = n // nx
    span = nz // 2
    chunks = part // LANES
    vmem = pl.BlockSpec(memory_space=pltpu.VMEM)
    hbm = pl.BlockSpec(memory_space=pltpu.HBM)
    bf16, f32 = jnp.bfloat16, jnp.float32
    ready = jax.ShapeDtypeStruct((width, units), bf16)
    dma = pltpu.SemaphoreType.DMA
    rows = (tok_rows, LANES)
    return pl.pallas_call(
        functools.partial(kernel, n, groups, nx, total_slots // 4),
        out_shape=(ready, ready, ready, jax.ShapeDtypeStruct((tok_rows, part), bf16)),
        in_specs=[hbm] * 7,
        out_specs=(vmem,) * 4,
        scratch_shapes=[
            pltpu.VMEM((DEPTH, source_rows, units), f32),
            pltpu.VMEM((tok_rows, width), bf16),
            pltpu.VMEM((1, source_rows), f32),
            pltpu.VMEM((source_rows, 1), f32),
            pltpu.VMEM((tok_rows, 1), f32),
            pltpu.VMEM((top_count, tok_rows), jnp.int32),
            pltpu.VMEM((top_count, tok_rows), bf16),
            pltpu.VMEM((3, n - 1, source_rows, units), bf16),
            pltpu.VMEM((n, tok_rows, part), bf16),
            pltpu.VMEM((n, 8, LANES), f32),
            pltpu.VMEM((n, 8, LANES), f32),
            pltpu.VMEM((n, tok_rows, capacity), bf16),
            pltpu.VMEM((groups, total_slots, part), bf16),
            pltpu.VMEM((total_slots, units), f32),
            pltpu.VMEM((total_slots, units), bf16),
            pltpu.VMEM((chunks, chips, total_slots, LANES), bf16),
            pltpu.VMEM((chunks, chips, total_slots, LANES), bf16),
            pltpu.VMEM((chunks, chips, total_slots, LANES), bf16),
            pltpu.VMEM((chunks, chips - 1, total_slots, LANES), bf16),
            pltpu.VMEM((total_slots, LANES), bf16),
            pltpu.VMEM((chunks, nz) + rows, f32),
            pltpu.VMEM((chunks, nx - 1, nz) + rows, bf16),
            pltpu.VMEM((chunks, nx - 1, nz) + rows, bf16),
            pltpu.VMEM((chunks, span - 1) + rows, bf16),
            pltpu.VMEM((chunks, span - 1) + rows, bf16),
            pltpu.VMEM((chunks, span) + rows, bf16),
            pltpu.VMEM((chunks, span, span) + rows, bf16),
            pltpu.VMEM((chunks, span) + rows, bf16),
            pltpu.VMEM((chunks,) + rows, bf16),
            pltpu.VMEM((tok_rows, part), bf16),
            dma((DEPTH,)),
            dma((5,)),
            dma,
            dma,
            dma,
            dma((span,)),
            dma((n,)),
            dma((chips,)),
            dma((chips,)),
            dma((chips,)),
            dma((chips,)),
            dma,
            dma((2,)),
            dma((chunks,)),
            dma,
            dma((chunks, nz)),
            dma,
            dma((chunks, chips, nz)),
            dma,
            dma((chunks, nx, nz)),
            dma,
            dma((chunks, span - 1)),
            dma,
            dma((chunks, span, span)),
            dma,
            dma((chunks,)),
        ],
        compiler_params=pltpu.CompilerParams(
            collective_id=0, has_side_effects=True, vmem_limit_bytes=44 * 1024 * 1024
        ),
    )(
        *(
            pltpu.with_memory_space_constraint(a, pltpu.HBM)
            for a in (tokens, gain, routes, route_weights, gate_local, up_local, down_local)
        )
    )


def body(tokens, norm_gain, gate_weight, up_weight, down_weight, routes, route_weights):
    gate_ready, up_ready, down_ready, moe_output = hand_over(
        tokens,
        norm_gain[None, :],
        routes.T,
        route_weights.T,
        gate_weight,
        up_weight,
        down_weight,
    )
    return settle(gate_ready[None], up_ready[None], down_ready[None], moe_output)


def solution(mesh):
    in_specs = (
        P("fs", None),
        P("fs"),
        P(None, "fs", "tp"),
        P(None, "fs", "tp"),
        P(None, "fs", "tp"),
        P("fs", None),
        P("fs", None),
    )
    out_specs = (P("fs", None, "tp"), P("fs", None, "tp"), P("fs", None, "tp"), P("fs", "tp"))
    return jax.shard_map(body, mesh=mesh, in_specs=in_specs, out_specs=out_specs, check_vma=False)
```

time: 222 us -> 184 us (0.83)
  Pallas kernels: 211 us -> 183 us
  local copies, waits for them, and re-layouts: 9.04 us -> 0 us
    pallas_call x1, Pallas kernels: 211 us -> 180 us  [hand_over(): pl.pallas_call(functools.partial(kernel, n, groups, nx, total_slots // 4)...]
    unnamed x10 -> x0, local copies, waits for them, and re-layouts: 7.57 us -> none
    pallas_call x0 -> x1, Pallas kernels: none -> 2.75 us  [settle(): pl.pallas_call(settle_kernel, out_shape=tuple((jax.ShapeDtypeStruct(a.sha...]
where the time goes in v2:
time: 184 us
  Pallas kernels  183 us (99%)
    pallas_call x1, Pallas kernels, hand_over(): pl.pallas_call(functools.partial(kernel, n, groups, nx, total_slots // 4)...  180 us

profile of v2, /device:TPU:0, one launch (start us, length us, event | category | flops | bytes accessed | tf_op | source)
XLA Modules:
  0.0 183.7 jit_solution(11818349348332196126)
XLA Ops:
  0.6 180.2 %shard_map.102 = (bf16[2048,512]{1,0:T(8,128)(2,1)S(1)}, bf16[2048,512]{1,0:T(8,128)(2,1)S(1)}, bf16[2048,512]{1,0:T(8,128)(2,1)S(1)}, bf16[256,512]{1,0:T(8,128)(2,1)S(1)}) custom-call(bf16[256,2048]{1,0:T(8,128)(2,1)} %tokens.1, f32[1,256]{1,0:T(1,128)} %bitcast.11, s32[4,256]{1,0:T(4,128)} %bitcast.9, bf16[4,256]{1,0:T(4,128)(2,1)} %bitcast.10, ...), custom_call_target="tpu_custom_call" | custom-call | tf_op jit(solution)/shard_map/pallas_call | solution.py:732
  180.8 2.8 %shard_map.103 = (bf16[1,2048,512]{2,1,0:T(8,128)(2,1)}, bf16[1,2048,512]{2,1,0:T(8,128)(2,1)}, bf16[1,2048,512]{2,1,0:T(8,128)(2,1)}, bf16[256,512]{1,0:T(8,128)(2,1)}) custom-call(bf16[1,2048,512]{2,1,0:T(8,128)(2,1)S(1)} %bitcast.6, bf16[1,2048,512]{2,1,0:T(8,128)(2,1)S(1)} %bitcast.7, bf16[1,2048,512]{2,1,0:T(8,128)(2,1)S(1)} %bitcast.8, ...), custom_call_target="tpu_custom_call" | custom-call | tf_op jit(solution)/shard_map/pallas_call | solution.py:702

commit v3 on v2

--- a/solution.py
+++ b/solution.py
@@ -530,7 +530,7 @@
                     kept.at[i, h, rows],
                     chip_sums.at[i, h - 1, rows],
                     chip_send,
-                    chip_recv.at[i, h, u],
+                    chip_recv.at[i, h - 1, u],
                     (me, lax.rem(chip + h, chips) * CORES + core),
                 )
 
@@ -558,7 +558,7 @@
                 x_out.at[i, dx - 1, u],
                 x_in.at[i, dx - 1, u],
                 x_send,
-                x_recv.at[i, dx, u],
+                x_recv.at[i, dx - 1, u],
                 (at(z, beside(dx)), tp),
             )
         row_sums[i, u] = rows_for(x)
@@ -632,24 +632,36 @@
             for u in which:
                 stage(i, u)
 
+    last = chunks - 1
+    near_units = range(span, nz)
     for step in range(chunks):
+        if step == last:
+            each(combine, step - 1, far_units)
         project(step)
-        each(spread, step - 2, all_units)
-        each(combine, step - 1, all_units)
-    last = chunks - 1
-    for u in all_units:
+        each(combine, step - 1, all_units if step < last else near_units)
+        each(spread, step - 2, far_units)
+        if step == last:
+            for i in range(last - 2):
+                each(cross, i, far_units)
+        each(spread, step - 2, near_units)
+    for u in far_units:
         combine(last, u)
-        if last > 0:
-            spread(last - 1, u)
-        if u == span - 1:
-            for i in range(last - 1):
-                each(cross, i, far_units)
-        if u >= span:
-            spread(last, u - span)
-    each(cross, last - 1, far_units)
-    for u in range(nz - span, nz):
-        cross(last, u - nz + span)
+        each(spread, last - 1, [u])
+        if u == 0:
+            each(cross, last - 2, far_units)
+    for u in near_units:
+        if u == nz - 1:
+            spread(last, 0)
+        combine(last, u)
+        if u - span < span:
+            each(cross, last - 1, [u - span])
+        each(spread, last - 1, [u] if u < nz - 1 else [])
+    for u in range(1, nz):
         spread(last, u)
+        if u == 1:
+            each(spread, last - 1, [nz - 1])
+        if u - 1 < span:
+            cross(last, u - 1)
     for i in range(chunks):
         finish(i)
 
@@ -782,9 +794,9 @@
             dma,
             dma((chunks, nz)),
             dma,
-            dma((chunks, chips, nz)),
-            dma,
-            dma((chunks, nx, nz)),
+            dma((chunks, chips - 1, nz)),
+            dma,
+            dma((chunks, nx - 1, nz)),
             dma,
             dma((chunks, span - 1)),
             dma,

time: 184 us -> 180 us (0.978)
  Pallas kernels: 183 us -> 179 us
    pallas_call x1, Pallas kernels: 180 us -> 176 us  [hand_over(): pl.pallas_call(functools.partial(kernel, n, groups, nx, total_slots // 4)...]
where the time goes in v3:
time: 180 us
  Pallas kernels  179 us (99%)
    pallas_call x1, Pallas kernels, hand_over(): pl.pallas_call(functools.partial(kernel, n, groups, nx, total_slots // 4)...  176 us

profile of v3, /device:TPU:0, one launch (start us, length us, event | category | flops | bytes accessed | tf_op | source)
XLA Modules:
  0.0 179.9 jit_solution(12466403977576503544)
XLA Ops:
  0.6 176.3 %shard_map.102 = (bf16[2048,512]{1,0:T(8,128)(2,1)S(1)}, bf16[2048,512]{1,0:T(8,128)(2,1)S(1)}, bf16[2048,512]{1,0:T(8,128)(2,1)S(1)}, bf16[256,512]{1,0:T(8,128)(2,1)S(1)}) custom-call(bf16[256,2048]{1,0:T(8,128)(2,1)} %tokens.1, f32[1,256]{1,0:T(1,128)} %bitcast.11, s32[4,256]{1,0:T(4,128)} %bitcast.9, bf16[4,256]{1,0:T(4,128)(2,1)} %bitcast.10, ...), custom_call_target="tpu_custom_call" | custom-call | tf_op jit(solution)/shard_map/pallas_call | solution.py:744
  177.0 2.8 %shard_map.103 = (bf16[1,2048,512]{2,1,0:T(8,128)(2,1)}, bf16[1,2048,512]{2,1,0:T(8,128)(2,1)}, bf16[1,2048,512]{2,1,0:T(8,128)(2,1)}, bf16[256,512]{1,0:T(8,128)(2,1)}) custom-call(bf16[1,2048,512]{2,1,0:T(8,128)(2,1)S(1)} %bitcast.6, bf16[1,2048,512]{2,1,0:T(8,128)(2,1)S(1)} %bitcast.7, bf16[1,2048,512]{2,1,0:T(8,128)(2,1)S(1)} %bitcast.8, ...), custom_call_target="tpu_custom_call" | custom-call | tf_op jit(solution)/shard_map/pallas_call | solution.py:714

commit v4 on v3

--- a/solution.py
+++ b/solution.py
@@ -644,24 +644,20 @@
             for i in range(last - 2):
                 each(cross, i, far_units)
         each(spread, step - 2, near_units)
-    for u in far_units:
+    each(spread, last - 1, far_units)
+    each(cross, last - 2, far_units)
+    for u in all_units:
+        if u > span:
+            spread(last, u - span - 1)
         combine(last, u)
-        each(spread, last - 1, [u])
-        if u == 0:
-            each(cross, last - 2, far_units)
-    for u in near_units:
-        if u == nz - 1:
-            spread(last, 0)
-        combine(last, u)
-        if u - span < span:
-            each(cross, last - 1, [u - span])
-        each(spread, last - 1, [u] if u < nz - 1 else [])
-    for u in range(1, nz):
+        if 0 < u <= span:
+            each(cross, last - 1, [u - 1])
+        if u < span:
+            each(spread, last - 1, [u + span])
+    for u in range(span - 1, nz):
         spread(last, u)
-        if u == 1:
-            each(spread, last - 1, [nz - 1])
-        if u - 1 < span:
-            cross(last, u - 1)
+        if u - span + 1 < span:
+            cross(last, u - span + 1)
     for i in range(chunks):
         finish(i)
 

time: 180 us -> 180 us (level)
  no operation moved by 1% of the time
where the time goes in v4:
time: 180 us; the launch traced here: 179 us
  Pallas kernels  179 us (99%)
    pallas_call x1, Pallas kernels, hand_over(): pl.pallas_call(functools.partial(kernel, n, groups, nx, total_slots // 4)...  176 us

profile of v4, /device:TPU:0, one launch (start us, length us, event | category | flops | bytes accessed | tf_op | source)
XLA Modules:
  0.0 179.5 jit_solution(6014761896795577906)
XLA Ops:
  0.6 175.9 %shard_map.102 = (bf16[2048,512]{1,0:T(8,128)(2,1)S(1)}, bf16[2048,512]{1,0:T(8,128)(2,1)S(1)}, bf16[2048,512]{1,0:T(8,128)(2,1)S(1)}, bf16[256,512]{1,0:T(8,128)(2,1)S(1)}) custom-call(bf16[256,2048]{1,0:T(8,128)(2,1)} %tokens.1, f32[1,256]{1,0:T(1,128)} %bitcast.11, s32[4,256]{1,0:T(4,128)} %bitcast.9, bf16[4,256]{1,0:T(4,128)(2,1)} %bitcast.10, ...), custom_call_target="tpu_custom_call" | custom-call | tf_op jit(solution)/shard_map/pallas_call | solution.py:740
  176.5 2.8 %shard_map.103 = (bf16[1,2048,512]{2,1,0:T(8,128)(2,1)}, bf16[1,2048,512]{2,1,0:T(8,128)(2,1)}, bf16[1,2048,512]{2,1,0:T(8,128)(2,1)}, bf16[256,512]{1,0:T(8,128)(2,1)}) custom-call(bf16[1,2048,512]{2,1,0:T(8,128)(2,1)S(1)} %bitcast.6, bf16[1,2048,512]{2,1,0:T(8,128)(2,1)S(1)} %bitcast.7, bf16[1,2048,512]{2,1,0:T(8,128)(2,1)S(1)} %bitcast.8, ...), custom_call_target="tpu_custom_call" | custom-call | tf_op jit(solution)/shard_map/pallas_call | solution.py:710

commit v5 on v4

--- a/solution.py
+++ b/solution.py
@@ -12,7 +12,7 @@
 gate_alpha = 1.702
 MESH = pl.DeviceIdType.MESH
 CORES = 2
-DEPTH = 6
+DEPTH = 8
 LANES = 128
 
 

time: 180 us -> 180 us (level)
  no operation moved by 1% of the time
where the time goes in v5:
time: 180 us; the launch traced here: 179 us
  Pallas kernels  179 us (99%)
    pallas_call x1, Pallas kernels, hand_over(): pl.pallas_call(functools.partial(kernel, n, groups, nx, total_slots // 4)...  176 us

profile of v5, /device:TPU:0, one launch (start us, length us, event | category | flops | bytes accessed | tf_op | source)
XLA Modules:
  0.0 179.5 jit_solution(16148556611640930062)
XLA Ops:
  0.6 175.9 %shard_map.102 = (bf16[2048,512]{1,0:T(8,128)(2,1)S(1)}, bf16[2048,512]{1,0:T(8,128)(2,1)S(1)}, bf16[2048,512]{1,0:T(8,128)(2,1)S(1)}, bf16[256,512]{1,0:T(8,128)(2,1)S(1)}) custom-call(bf16[256,2048]{1,0:T(8,128)(2,1)} %tokens.1, f32[1,256]{1,0:T(1,128)} %bitcast.11, s32[4,256]{1,0:T(4,128)} %bitcast.9, bf16[4,256]{1,0:T(4,128)(2,1)} %bitcast.10, ...), custom_call_target="tpu_custom_call" | custom-call | tf_op jit(solution)/shard_map/pallas_call | solution.py:740
  176.6 2.8 %shard_map.103 = (bf16[1,2048,512]{2,1,0:T(8,128)(2,1)}, bf16[1,2048,512]{2,1,0:T(8,128)(2,1)}, bf16[1,2048,512]{2,1,0:T(8,128)(2,1)}, bf16[256,512]{1,0:T(8,128)(2,1)}) custom-call(bf16[1,2048,512]{2,1,0:T(8,128)(2,1)S(1)} %bitcast.6, bf16[1,2048,512]{2,1,0:T(8,128)(2,1)S(1)} %bitcast.7, bf16[1,2048,512]{2,1,0:T(8,128)(2,1)S(1)} %bitcast.8, ...), custom_call_target="tpu_custom_call" | custom-call | tf_op jit(solution)/shard_map/pallas_call | solution.py:710
